TPU v7x, 512 devices: a whole 4x4x16 slice. The times are simulated.
512 devices in a mesh: kv: 16 (over y, x), tp: 32 (over z, core).
Axes of the slice: x: 4, y: 4, z: 16, core: 2. Of those that a mesh axis runs over, the one named last changes fastest.
Arguments:
- tokens: bfloat16 [3, 4096], P(None, ('kv', 'tp')), may hold values from -40 to 40
- lengths: int32 [3], replicated, may hold values from 1 to 131072, as said below
- attn_gain: float32 [4096], P(('kv', 'tp')), may hold values from 0.1 to 1.9
- w_query: bfloat16 [4096, 2048], P('kv', 'tp'), may hold values from -0.09375 to 0.09375
- w_key: bfloat16 [4096, 128], P('kv'), may hold values from -0.09375 to 0.09375
- w_value: bfloat16 [4096, 128], P('kv'), may hold values from -0.09375 to 0.09375
- w_forget: bfloat16 [4096, 32], replicated, may hold values from -0.09375 to 0.09375
- forget_bias: float32 [32], replicated, may hold values from -4 to 0
- cache_keys: bfloat16 [3, 128, 131072], P(None, None, ('kv', 'tp')), may hold values from -320 to 320
- cache_values: bfloat16 [3, 128, 131072], P(None, None, ('kv', 'tp')), may hold values from -6 to 6
- cache_decay: float32 [3, 32, 131072], P(None, None, ('kv', 'tp')), may hold values from -16388 to 0, as said below
- out_gain: float32 [2048], replicated, may hold values from 0.1 to 1.9
- w_out: bfloat16 [2048, 4096], P('tp', 'kv'), may hold values from -0.125 to 0.125
- mlp_gain: float32 [4096], P(('kv', 'tp')), may hold values from 0.1 to 1.9
- w_gate: bfloat16 [4096, 11264], P('kv', 'tp'), may hold values from -0.09375 to 0.09375
- w_up: bfloat16 [4096, 11264], P('kv', 'tp'), may hold values from -0.09375 to 0.09375
- w_down: bfloat16 [11264, 4096], P('tp', 'kv'), may hold values from -0.0546875 to 0.0546875
Outputs:
- layer_out: bfloat16 [3, 4096], P(None, ('kv', 'tp'))
Inputs may be any that keep to these rules, and one draw needn't show every extreme that they name: Sequence b has lengths[b] live cache positions, 0 to lengths[b] - 1; some sequence has exactly 131072 in every draw. On live positions, cache_decay[b, h, j] is the sum of the log forget gates of sequence b and head h over positions j + 1 to lengths[b] - 1, so it is zero at the last live position and never rises toward earlier positions; it is zero beyond lengths[b].
All inputs are finite; a program needn't handle non-finite values.
Results may differ from a plain program's by a relative error of at most 0.013.
Values may be sent and summed in bfloat16 or wider, within the bound.
A program may use at most 64 MiB of HBM per device.

v0:
```python
import jax
import jax.numpy as jnp
from jax import lax
from jax.sharding import Mesh
from jax.sharding import PartitionSpec as P

QUERY_HEAD_COUNT = 32
HD = 64
KV_HEADS = 2
TP = ("tp_0", "tp_1")
KV = ("kv_0", "kv_1")
KV_TP = ("kv_0", "kv_1", "tp_0", "tp_1")


epsilon = 1e-06
masked_score = -1e30


def sent_to_all(x, axis):
    copies = jnp.broadcast_to(x, (lax.axis_size(axis), *x.shape))
    return lax.all_to_all(copies, axis, split_axis=0, concat_axis=0, tiled=True)


def joined_along(blocks, dim):
    lengths = list(blocks.shape[1:])
    lengths[dim] *= blocks.shape[0]
    return jnp.moveaxis(blocks, 0, dim).reshape(lengths)


def collect(x, axis, dim):
    blocks = sent_to_all(x, axis)
    return joined_along(blocks, dim)


def by_axis(x, axes):
    for axis in axes:
        x = lax.psum(x, axis)
    return x


def all_in_one(x, axis):
    leaves = jax.tree.leaves(x)
    turns = sorted(range(len(leaves)), key=lambda k: -leaves[k].size)
    width = (1, *leaves[turns[0]].shape)[-1]
    lines = [
        jnp.pad(leaves[k].reshape(-1), (0, -leaves[k].size % width)).reshape(-1, width)
        for k in turns
    ]
    both, at, found = (lax.all_gather(jnp.concatenate(lines), axis), 0, {})
    for k, line in zip(turns, lines):
        piece = both[:, at : at + len(line)].reshape(len(both), -1)
        found[k] = piece[:, : leaves[k].size].reshape(-1, *leaves[k].shape)
        at += len(line)
    numbers = iter(range(len(leaves)))
    return jax.tree.map(lambda _: found[next(numbers)], x)


def merged_by_axis(x, axes, combine):
    for axis in axes:
        pieces = all_in_one(x, axis)
        x = jax.tree.map(lambda part: part[0], pieces)
        for k in range(1, lax.axis_size(axis)):
            x = combine(x, jax.tree.map(lambda part: part[k], pieces))
    return x


def in_blocks(x, dim, length):
    lengths = x.shape
    blocks = x.reshape(*lengths[:dim], length, lengths[dim] // length, *lengths[dim + 1 :])
    return jnp.moveaxis(blocks, dim, 0)


def summed_on_arrival(x, axis, dim):
    length = lax.axis_size(axis)
    blocks = lax.all_to_all(in_blocks(x, dim, length), axis, 0, 0, tiled=True)
    return jnp.sum(blocks, axis=0)


def spread_rows(share, gain):
    scaled = (share.astype(jnp.float32) * gain).astype(jnp.bfloat16)
    squares = jnp.sum(jnp.square(share.astype(jnp.float32)), axis=1)
    row_block, square_parts = (
        collect(scaled.astype(jnp.float32), TP, 1).astype(scaled.dtype),
        collect(squares[:, None], TP, 1),
    )
    square_total = jnp.sum(square_parts, axis=1)
    return (row_block, square_total)


def combine_partials(earlier, later):
    top_a, total_a, sums_a = earlier
    top_b, total_b, sums_b = later
    score_top = jnp.maximum(top_a, top_b)
    scale_a = jnp.exp(top_a - score_top)
    scale_b = jnp.exp(top_b - score_top)
    return (
        score_top,
        total_a * scale_a + total_b * scale_b,
        sums_a * scale_a[..., None] + sums_b * scale_b[..., None],
    )


def body(
    tokens,
    lengths,
    attn_gain,
    w_query,
    w_key,
    w_value,
    w_forget,
    forget_bias,
    cache_keys,
    cache_values,
    cache_decay,
    out_gain,
    w_out,
    mlp_gain,
    w_gate,
    w_up,
    w_down,
):
    full_width = tokens.shape[1] * lax.axis_size(KV) * lax.axis_size(TP)
    kv_index = lax.axis_index(KV)
    tp_index = lax.axis_index(TP)
    row_block, square_total = spread_rows(tokens, attn_gain)
    block_rows = row_block.shape[1]
    forget_rows = lax.dynamic_slice_in_dim(w_forget, kv_index * block_rows, block_rows, 0)
    query_part = jnp.dot(row_block, w_query, preferred_element_type=jnp.float32)
    key_part = jnp.dot(row_block, w_key, preferred_element_type=jnp.float32)
    value_part = jnp.dot(row_block, w_value, preferred_element_type=jnp.float32)
    forget_part = jnp.dot(row_block, forget_rows, preferred_element_type=jnp.float32)
    query_sum, key_sum, value_sum, forget_sum, square_total = (
        by_axis(query_part, KV),
        by_axis(key_part, KV),
        by_axis(value_part, KV),
        by_axis(forget_part, KV),
        by_axis(square_total, KV),
    )
    first_rms = lax.rsqrt(square_total / full_width + epsilon)[:, None]
    query_local = (query_sum * first_rms).astype(jnp.bfloat16)
    key_new = (key_sum * first_rms).astype(jnp.bfloat16)
    value_new = (value_sum * first_rms).astype(jnp.bfloat16)
    log_gate = jax.nn.log_sigmoid(forget_sum * first_rms + forget_bias)
    query_all = collect(query_local, TP, 1)
    batch_rows, key_dims, span = cache_keys.shape
    groups = QUERY_HEAD_COUNT // KV_HEADS
    score_scale = HD ** (-0.5)
    query_grouped = query_all.reshape(batch_rows, KV_HEADS, groups, HD)
    keys_grouped = cache_keys.reshape(batch_rows, KV_HEADS, HD, span)
    values_grouped = cache_values.reshape(batch_rows, KV_HEADS, HD, span)
    scores = jnp.einsum(
        "bkgd,bkdj->bkgj", query_grouped, keys_grouped, preferred_element_type=jnp.float32
    ).reshape(batch_rows, QUERY_HEAD_COUNT, span)
    scores = scores * score_scale + cache_decay + log_gate[:, :, None]
    first_slot = (kv_index * lax.axis_size(TP) + tp_index) * span
    token_positions = first_slot + lax.iota(jnp.int32, span)
    is_live = (token_positions[None, :] < lengths[:, None])[:, None, :]
    scores = jnp.where(is_live, scores, masked_score)
    own_score = (
        jnp.einsum(
            "inpo,ino->inp",
            query_grouped,
            key_new.reshape(batch_rows, KV_HEADS, HD),
            preferred_element_type=jnp.float32,
        ).reshape(batch_rows, QUERY_HEAD_COUNT)
        * score_scale
    )
    local_top = jnp.maximum(jnp.max(scores, axis=2), own_score)
    head_count = w_out.shape[0] // HD
    head_start = tp_index * head_count
    weights = jnp.where(is_live, jnp.exp(scores - local_top[:, :, None]), 0.0)
    weight_total = jnp.sum(weights, axis=2)
    rounded = weights.astype(jnp.bfloat16).reshape(batch_rows, KV_HEADS, groups, span)
    value_sums = jnp.einsum(
        "bkgj,bkdj->bkgd", rounded, values_grouped, preferred_element_type=jnp.float32
    ).reshape(batch_rows, QUERY_HEAD_COUNT, HD)
    weight_total, value_sums = (weight_total, value_sums)
    score_top, weight_total, value_sums = merged_by_axis(
        (local_top, weight_total, value_sums), KV_TP, combine_partials
    )
    weight_total = lax.dynamic_slice_in_dim(weight_total, head_start, head_count, 1)
    value_sums = lax.dynamic_slice_in_dim(value_sums, head_start, head_count, 1)
    score_top = lax.dynamic_slice_in_dim(score_top, head_start, head_count, 1)
    own_here = lax.dynamic_slice_in_dim(own_score, head_start, head_count, 1)
    new_values = jnp.repeat(value_new.reshape(batch_rows, KV_HEADS, HD), groups, axis=1)
    new_values = lax.dynamic_slice_in_dim(new_values, head_start, head_count, 1).astype(jnp.float32)
    own_weight = jnp.exp(own_here - score_top)
    heads_out = (value_sums + own_weight[:, :, None] * new_values) / (weight_total + own_weight)[
        :, :, None
    ]
    head_gains = lax.dynamic_slice_in_dim(out_gain, head_start * HD, head_count * HD, 0).reshape(
        head_count, HD
    )
    normed = (
        heads_out
        * lax.rsqrt(jnp.mean(jnp.square(heads_out), axis=2, keepdims=True) + epsilon)
        * head_gains
    )
    normed = normed.astype(jnp.bfloat16).reshape(batch_rows, head_count * HD)
    attn_part = jnp.dot(normed, w_out, preferred_element_type=jnp.float32)
    attn_share = summed_on_arrival(attn_part, TP, 1)
    residual = (tokens.astype(jnp.float32) + attn_share).astype(jnp.bfloat16)
    mlp_block, mlp_squares = spread_rows(residual, mlp_gain)
    gate_part = jnp.dot(mlp_block, w_gate, preferred_element_type=jnp.float32)
    up_part = jnp.dot(mlp_block, w_up, preferred_element_type=jnp.float32)
    gate_sum, up_sum, mlp_squares = (
        by_axis(gate_part, KV),
        by_axis(up_part, KV),
        by_axis(mlp_squares, KV),
    )
    second_rms = lax.rsqrt(mlp_squares / full_width + epsilon)[:, None]
    hidden = (jax.nn.silu(gate_sum * second_rms) * (up_sum * second_rms)).astype(jnp.bfloat16)
    down_part = jnp.dot(hidden, w_down, preferred_element_type=jnp.float32)
    mlp_share = summed_on_arrival(down_part, TP, 1)
    return (residual.astype(jnp.float32) + mlp_share).astype(jnp.bfloat16)


def solution(mesh):
    torus = Mesh(mesh.devices.reshape(4, 4, 16, 2), ("kv_0", "kv_1", "tp_0", "tp_1"))
    placed = (
        P(None, KV_TP),
        P(),
        P(KV_TP),
        P(KV, TP),
        P(KV, None),
        P(KV, None),
        P(),
        P(),
        P(None, None, KV_TP),
        P(None, None, KV_TP),
        P(None, None, KV_TP),
        P(),
        P(TP, KV),
        P(KV_TP),
        P(KV, TP),
        P(KV, TP),
        P(TP, KV),
    )
    return jax.shard_map(
        body, mesh=torus, in_specs=placed, out_specs=P(None, KV_TP), check_vma=False
    )
```

profile of v0, /device:TPU:1, one launch (start us, length us, event | category | flops | bytes accessed | tf_op | source)
XLA Modules:
  0.0 252.3 jit_solution(7297757308476043918)
XLA Ops:
  0.0 0.8 copy.80
  0.9 0.6 broadcast_in_dim.32
  1.5 16.7 %all-to-all-start.1 = ((f32[32,3,1]{1,2,0:T(1,128)}), f32[32,3,1]{1,2,0:T(1,128)S(1)}, u32[]{:S(2)}, u32[]{:S(2)}) async-start(f32[32,3,1]{1,2,0:T(1,128)} %broadcast_in_dim.32), calls=%async_computation.1 | async-start | bytes 32768 | tf_op jit(solution)/shard_map/all_to_all | solution.py:21
  18.4 11.6 %all-to-all-done.1 = f32[32,3,1]{1,2,0:T(1,128)S(1)} async-done(((f32[32,3,1]{1,2,0:T(1,128)}), f32[32,3,1]{1,2,0:T(1,128)S(1)}, u32[]{:S(2)}, u32[]{:S(2)}) %all-to-all-start.1) | async-done | bytes 416 | tf_op jit(solution)/shard_map/all_to_all | solution.py:21
  30.0 0.6 broadcast_in_dim.31
  30.6 4.6 %all-to-all-start = ((bf16[32,3,8]{2,1,0:T(4,128)(2,1)}), bf16[32,3,8]{2,1,0:T(4,128)(2,1)S(1)}, u32[]{:S(2)}, u32[]{:S(2)}) async-start(bf16[32,3,8]{2,1,0:T(4,128)(2,1)} %broadcast_in_dim.31), calls=%async_computation | async-start | bytes 65536 | tf_op jit(solution)/shard_map/all_to_all | solution.py:21
  35.4 0.8 dynamic_slice.27
  36.2 11.2 %all-to-all-done = bf16[32,3,8]{2,1,0:T(4,128)(2,1)S(1)} async-done(((bf16[32,3,8]{2,1,0:T(4,128)(2,1)}), bf16[32,3,8]{2,1,0:T(4,128)(2,1)S(1)}, u32[]{:S(2)}, u32[]{:S(2)}) %all-to-all-start) | async-done | bytes 1568 | tf_op jit(solution)/shard_map/all_to_all | solution.py:21
  47.8 0.5 copy-done.7
  48.6 8.9 %all-reduce.11 = (f32[3,128]{1,0:T(4,128)S(1)}, f32[3]{0:T(128)S(1)}, f32[3,64]{1,0:T(4,128)S(1)}, f32[3,32]{1,0:T(4,128)S(1)}, f32[3,128]{1,0:T(4,128)S(1)}) all-reduce(f32[3,128]{1,0:T(4,128)S(1)} %fusion.204, f32[3]{0:T(128)S(1)} %reduce_sum.73, ...), channel_id=1, replica_groups=mesh['kv_0'=4,'kv_1'=4,'tp_0'=16,'tp_1'=2] {'kv_0'}, use_global_device_ids=true, to_apply=%region_12.13 | all-reduce | flops 1059 | bytes 8472 | tf_op jit(solution)/shard_map/psum | solution.py:37
  57.5 8.7 %all-reduce.9 = (f32[3,128]{1,0:T(4,128)S(1)}, f32[3]{0:T(128)S(1)}, f32[3,64]{1,0:T(4,128)S(1)}, f32[3,32]{1,0:T(4,128)S(1)}, f32[3,128]{1,0:T(4,128)S(1)}) all-reduce(f32[3,128]{1,0:T(4,128)S(1)} %get-tuple-element.22, f32[3]{0:T(128)S(1)} %get-tuple-element.23, ...), channel_id=1, replica_groups=mesh['kv_0'=4,'kv_1'=4,'tp_0'=16,'tp_1'=2] {'kv_1'}, use_global_device_ids=true, to_apply=%region_13.14 | all-reduce | flops 1059 | bytes 8472 | tf_op jit(solution)/shard_map/psum | solution.py:37
  66.3 0.6 broadcast_in_dim.33
  66.9 8.6 %all-to-all-start.2 = ((bf16[32,3,64]{2,1,0:T(4,128)(2,1)}), bf16[32,3,64]{2,1,0:T(4,128)(2,1)S(1)}, u32[]{:S(2)}, u32[]{:S(2)}) async-start(bf16[32,3,64]{2,1,0:T(4,128)(2,1)} %broadcast_in_dim.33), calls=%async_computation.2 | async-start | bytes 65536 | tf_op jit(solution)/shard_map/all_to_all | solution.py:21
  75.5 0.7 copy-done.12
  76.4 11.3 %all-to-all-done.2 = bf16[32,3,64]{2,1,0:T(4,128)(2,1)S(1)} async-done(((bf16[32,3,64]{2,1,0:T(4,128)(2,1)}), bf16[32,3,64]{2,1,0:T(4,128)(2,1)S(1)}, u32[]{:S(2)}, u32[]{:S(2)}) %all-to-all-start.2) | async-done | bytes 12320 | tf_op jit(solution)/shard_map/all_to_all | solution.py:21
  88.2 0.8 copy-done.5
  89.4 0.6 copy-done.2
  90.8 9.1 %all-gather.4 = f32[4,100,64]{1,2,0:T(8,128)S(1)} all-gather(f32[1,100,64]{1,2,0:T(8,128)S(1)} %maximum_bitcast_fusion), channel_id=2, replica_groups=mesh['kv_0'=4,'kv_1'=4,'tp_0'=16,'tp_1'=2] {'kv_0'}, dimensions={0}, use_global_device_ids=true | all-gather | bytes 128000 | tf_op jit(solution)/shard_map/all_gather | solution.py:49
  100.9 9.1 %all-gather.5 = f32[4,100,64]{1,2,0:T(8,128)S(1)} all-gather(f32[1,100,64]{1,2,0:T(8,128)S(1)} %maximum_bitcast_fusion.1), channel_id=3, replica_groups=mesh['kv_0'=4,'kv_1'=4,'tp_0'=16,'tp_1'=2] {'kv_1'}, dimensions={0}, use_global_device_ids=true | all-gather | bytes 128000 | tf_op jit(solution)/shard_map/all_gather | solution.py:49
  111.0 22.9 %all-gather.6 = f32[16,100,64]{1,2,0:T(8,128)S(1)} all-gather(f32[1,100,64]{1,2,0:T(8,128)S(1)} %maximum_bitcast_fusion.2), channel_id=4, replica_groups=mesh['kv_0'=4,'kv_1'=4,'tp_0'=16,'tp_1'=2] {'tp_0'}, dimensions={0}, use_global_device_ids=true | all-gather | bytes 435200 | tf_op jit(solution)/shard_map/all_gather | solution.py:49
  135.5 15.0 %all-gather.7 = f32[2,100,64]{1,2,0:T(8,128)S(1)} all-gather(f32[1,100,64]{1,2,0:T(8,128)S(1)} %maximum_bitcast_fusion.3), channel_id=5, replica_groups=mesh['kv_0'=4,'kv_1'=4,'tp_0'=16,'tp_1'=2] {'tp_1'}, dimensions={0}, use_global_device_ids=true | all-gather | bytes 76800 | tf_op jit(solution)/shard_map/all_gather | solution.py:49
  152.5 17.7 %all_to_all.35 = f32[32,3,8]{2,1,0:T(4,128)S(1)} all-to-all(f32[32,3,8]{2,1,0:T(4,128)S(1)} %copy.105), channel_id=1, replica_groups=mesh['kv_0'=4,'kv_1'=4,'tp_0'=16,'tp_1'=2] {'tp_0','tp_1'}, dimensions={0} | all-to-all | bytes 6144 | tf_op jit(solution)/shard_map/all_to_all | solution.py:75
  170.4 0.6 broadcast_in_dim.38
  171.0 5.1 %all-to-all-start.5 = ((f32[32,3,1]{1,2,0:T(1,128)}), f32[32,3,1]{1,2,0:T(1,128)S(1)}, u32[]{:S(2)}, u32[]{:S(2)}) async-start(f32[32,3,1]{1,2,0:T(1,128)} %broadcast_in_dim.38), calls=%async_computation.5 | async-start | bytes 32768 | tf_op jit(solution)/shard_map/all_to_all | solution.py:21
  176.3 11.7 %all-to-all-done.5 = f32[32,3,1]{1,2,0:T(1,128)S(1)} async-done(((f32[32,3,1]{1,2,0:T(1,128)}), f32[32,3,1]{1,2,0:T(1,128)S(1)}, u32[]{:S(2)}, u32[]{:S(2)}) %all-to-all-start.5) | async-done | bytes 416 | tf_op jit(solution)/shard_map/all_to_all | solution.py:21
  188.0 0.6 broadcast_in_dim.37
  188.6 4.5 %all-to-all-start.4 = ((bf16[32,3,8]{2,1,0:T(4,128)(2,1)}), bf16[32,3,8]{2,1,0:T(4,128)(2,1)S(1)}, u32[]{:S(2)}, u32[]{:S(2)}) async-start(bf16[32,3,8]{2,1,0:T(4,128)(2,1)} %broadcast_in_dim.37), calls=%async_computation.4 | async-start | bytes 65536 | tf_op jit(solution)/shard_map/all_to_all | solution.py:21
  193.2 12.2 %all-to-all-done.4 = bf16[32,3,8]{2,1,0:T(4,128)(2,1)S(1)} async-done(((bf16[32,3,8]{2,1,0:T(4,128)(2,1)}), bf16[32,3,8]{2,1,0:T(4,128)(2,1)S(1)}, u32[]{:S(2)}, u32[]{:S(2)}) %all-to-all-start.4) | async-done | bytes 1568 | tf_op jit(solution)/shard_map/all_to_all | solution.py:21
  205.8 10.8 %all-reduce.10 = (f32[3,352]{1,0:T(4,128)S(1)}, f32[3,352]{1,0:T(4,128)S(1)}, f32[3]{0:T(128)S(1)}) all-reduce(f32[3,352]{1,0:T(4,128)S(1)} %fusion.206, f32[3,352]{1,0:T(4,128)S(1)} %fusion.205, f32[3]{0:T(128)S(1)} %reduce_sum.78), channel_id=1, replica_groups=mesh['kv_0'=4,'kv_1'=4,'tp_0'=16,'tp_1'=2] {'kv_0'}, use_global_device_ids=true, to_apply=%region_22.23 | all-reduce | flops 2115 | bytes 16920 | tf_op jit(solution)/shard_map/psum | solution.py:37
  216.7 11.1 %all-reduce.8 = (f32[3,352]{1,0:T(4,128)S(1)}, f32[3,352]{1,0:T(4,128)S(1)}, f32[3]{0:T(128)S(1)}) all-reduce(f32[3,352]{1,0:T(4,128)S(1)} %get-tuple-element.19, f32[3,352]{1,0:T(4,128)S(1)} %get-tuple-element.20, f32[3]{0:T(128)S(1)} %get-tuple-element.21), channel_id=1, replica_groups=mesh['kv_0'=4,'kv_1'=4,'tp_0'=16,'tp_1'=2] {'kv_1'}, use_global_device_ids=true, to_apply=%region_23.24 | all-reduce | flops 2115 | bytes 16920 | tf_op jit(solution)/shard_map/psum | solution.py:37
  228.2 23.3 %all_to_all.36 = f32[32,3,8]{2,1,0:T(4,128)S(1)} all-to-all(f32[32,3,8]{2,1,0:T(4,128)S(1)} %copy.109), channel_id=1, replica_groups=mesh['kv_0'=4,'kv_1'=4,'tp_0'=16,'tp_1'=2] {'tp_0','tp_1'}, dimensions={0} | all-to-all | bytes 6144 | tf_op jit(solution)/shard_map/all_to_all | solution.py:75
  251.7 0.7 copy.111
  (149 shorter events, 9.9 us)
Async XLA Ops:
  0.0 48.4 %copy-start = (bf16[4096,32]{0,1:T(8,128)(2,1)S(1)}, bf16[4096,32]{0,1:T(8,128)(2,1)}, u32[]{:S(2)}) copy-start(bf16[4096,32]{0,1:T(8,128)(2,1)} %param.23) | copy-start | bytes 786436
  0.0 0.8 copy-start.10
  1.5 28.5 %all-to-all-start.1 = ((f32[32,3,1]{1,2,0:T(1,128)}), f32[32,3,1]{1,2,0:T(1,128)S(1)}, u32[]{:S(2)}, u32[]{:S(2)}) async-start(f32[32,3,1]{1,2,0:T(1,128)} %broadcast_in_dim.32), calls=%async_computation.1 | async-start | bytes 32768 | tf_op jit(solution)/shard_map/all_to_all | solution.py:21
  30.6 4.6 %copy-start.11 = (s32[3]{0:T(128)S(1)}, s32[3]{0:T(128)}, u32[]{:S(2)}) copy-start(s32[3]{0:T(128)} %param.18) | copy-start | bytes 40
  30.6 4.7 %copy-start.8 = (bf16[64,256]{1,0:T(8,128)(2,1)S(1)}, bf16[64,256]{1,0:T(8,128)(2,1)}, u32[]{:S(2)}) copy-start(bf16[64,256]{1,0:T(8,128)(2,1)} %param.29) | copy-start | bytes 98308
  30.6 16.8 %all-to-all-start = ((bf16[32,3,8]{2,1,0:T(4,128)(2,1)}), bf16[32,3,8]{2,1,0:T(4,128)(2,1)S(1)}, u32[]{:S(2)}, u32[]{:S(2)}) async-start(bf16[32,3,8]{2,1,0:T(4,128)(2,1)} %broadcast_in_dim.31), calls=%async_computation | async-start | bytes 65536 | tf_op jit(solution)/shard_map/all_to_all | solution.py:21
  36.2 11.4 %copy-start.9 = (bf16[256,64]{0,1:T(8,128)(2,1)S(1)}, bf16[256,64]{0,1:T(8,128)(2,1)}, u32[]{:S(2)}) copy-start(bf16[256,64]{0,1:T(8,128)(2,1)} %param.20) | copy-start | bytes 98308
  36.2 11.5 %copy-start.6 = (bf16[256,128]{1,0:T(8,128)(2,1)S(1)}, bf16[256,128]{1,0:T(8,128)(2,1)}, u32[]{:S(2)}) copy-start(bf16[256,128]{1,0:T(8,128)(2,1)} %param.21) | copy-start | bytes 196612
  47.5 0.8 copy-start.7
  48.3 39.7 %copy-start.1 = (bf16[3,128,256]{2,1,0:T(8,128)(2,1)S(1)}, bf16[3,128,256]{2,1,0:T(8,128)(2,1)}, u32[]{:S(2)}) copy-start(bf16[3,128,256]{2,1,0:T(8,128)(2,1)} %param.25) | copy-start | bytes 589828
  66.9 20.8 %all-to-all-start.2 = ((bf16[32,3,64]{2,1,0:T(4,128)(2,1)}), bf16[32,3,64]{2,1,0:T(4,128)(2,1)S(1)}, u32[]{:S(2)}, u32[]{:S(2)}) async-start(bf16[32,3,64]{2,1,0:T(4,128)(2,1)} %broadcast_in_dim.33), calls=%async_computation.2 | async-start | bytes 65536 | tf_op jit(solution)/shard_map/all_to_all | solution.py:21
  75.5 0.7 copy-start.12
  88.0 0.9 copy-start.5
  89.0 0.9 copy-start.2
  152.5 23.6 %copy-start.13 = (f32[8]{0:T(128)S(1)}, f32[8]{0:T(128)}, u32[]{:S(2)}) copy-start(f32[8]{0:T(128)} %param.30) | copy-start | bytes 100
  170.2 35.3 %copy-start.3 = (bf16[256,352]{0,1:T(8,128)(2,1)S(1)}, bf16[256,352]{0,1:T(8,128)(2,1)}, u32[]{:S(2)}) copy-start(bf16[256,352]{0,1:T(8,128)(2,1)} %param.31) | copy-start | bytes 540676
  171.0 17.0 %all-to-all-start.5 = ((f32[32,3,1]{1,2,0:T(1,128)}), f32[32,3,1]{1,2,0:T(1,128)S(1)}, u32[]{:S(2)}, u32[]{:S(2)}) async-start(f32[32,3,1]{1,2,0:T(1,128)} %broadcast_in_dim.38), calls=%async_computation.5 | async-start | bytes 32768 | tf_op jit(solution)/shard_map/all_to_all | solution.py:21
  188.6 17.0 %copy-start.4 = (bf16[256,352]{0,1:T(8,128)(2,1)S(1)}, bf16[256,352]{0,1:T(8,128)(2,1)}, u32[]{:S(2)}) copy-start(bf16[256,352]{0,1:T(8,128)(2,1)} %param.32) | copy-start | bytes 540676
  188.6 16.8 %all-to-all-start.4 = ((bf16[32,3,8]{2,1,0:T(4,128)(2,1)}), bf16[32,3,8]{2,1,0:T(4,128)(2,1)S(1)}, u32[]{:S(2)}, u32[]{:S(2)}) async-start(bf16[32,3,8]{2,1,0:T(4,128)(2,1)} %broadcast_in_dim.37), calls=%async_computation.4 | async-start | bytes 65536 | tf_op jit(solution)/shard_map/all_to_all | solution.py:21
  205.5 22.3 %copy-start.14 = (bf16[352,256]{1,0:T(8,128)(2,1)S(1)}, bf16[352,256]{1,0:T(8,128)(2,1)}, u32[]{:S(2)}) copy-start(bf16[352,256]{1,0:T(8,128)(2,1)} %param.33) | copy-start | bytes 540676
where the time goes:
time: 253 us; the launch traced here: 252 us
  blocking collectives  137 us (54%)
  waiting for transfers between devices  58.1 us (23%)
  starting transfers between devices  39.5 us (16%)
  local copies, waits for them, and re-layouts  13.8 us (5%)
    all_to_all x5, waiting for transfers between devices, sent_to_all(): return lax.all_to_all(copies, axis, split_axis=0, concat_axis=0, tiled=True)  58.1 us
    all_gather x4, blocking collectives, all_in_one(): both, at, found = (lax.all_gather(jnp.concatenate(lines), axis), 0, {})  56.1 us
    all_to_all x2, blocking collectives, summed_on_arrival(): blocks = lax.all_to_all(in_blocks(x, dim, length), axis, 0, 0, tiled=True)  41.1 us
    psum x4, blocking collectives, by_axis(): x = lax.psum(x, axis)  39.6 us
    all_to_all x5, starting transfers between devices, sent_to_all(): return lax.all_to_all(copies, axis, split_axis=0, concat_axis=0, tiled=True)  39.5 us
  transfers between devices with their start and end apart: 5, of which 5 were waited for; matrix products, arithmetic and copies ran while one was open for 1% of the time, Pallas kernels for 0%

commit v1 on v0

v1 whole, which is shorter than its diff:
```python
import jax
import jax.numpy as jnp
from jax import lax
from jax.experimental import pallas as pl
from jax.experimental.pallas import tpu as pltpu
from jax.sharding import PartitionSpec as P

MESH = pl.DeviceIdType.MESH
D = 4096
HD = 64
NTP = 32
NKV = 16
FF_DEV = 352
FF_PAD = 384
SPAN = 256
EPS = 1e-06
MASKED = -1e30
F32 = jnp.float32
BF16 = jnp.bfloat16

NT = (((1,), (1,)), ((), ()))
NN = (((1,), (0,)), ((), ()))

Z_ORDER = [8, 7, -7, 6, -6, 5, -5, 4, -4, 3, -3, 2, -2, 1, -1]


def dot(a, b, dims, **kw):
    return lax.dot_general(a, b, dims, preferred_element_type=F32, **kw)


def iota(shape, dim):
    return lax.broadcasted_iota(jnp.int32, shape, dim)


def kernel(
    lengths, tokens, attn_gain, mlp_gain, forget_bias, out_gain,
    w_query, w_key, w_value, w_forget, keys, values, decay, w_out,
    w_gate, w_up, w_down,
    out,
    tok_v, ag_v, mg_v, fb_v, og_v, wqf, wk, wv, wkv, k_v, v_v, d_v, wo,
    wg, wu, wd,
    buf1, buf2, buf3, stage4, buf4, buf5, buf6, buf7, stage8, buf8,
    lsem, ssem, rsem,
):
    kv = lax.axis_index("kv")
    tp = lax.axis_index("tp")
    g = tp // 16
    z = tp // 2
    core = tp % 2
    y = kv // 4
    x = kv % 4

    def load(i, src, dst):
        c = pltpu.make_async_copy(src, dst, lsem.at[i])
        c.start()
        return c

    half = pl.multiple_of(g * HD, HD)
    other = pl.multiple_of((1 - g) * HD, HD)
    c_tok = load(0, tokens, tok_v)
    c_ag = load(1, attn_gain, ag_v)
    c_mg = load(2, mlp_gain, mg_v)
    c_wq = load(3, w_query, wqf.at[pl.ds(half, HD)])
    cols = pl.ds(pl.multiple_of(kv * 256, 256), 256)
    c_wf = load(4, w_forget.at[:, cols], wqf.at[pl.ds(other, 32)])
    c_wk = load(5, w_key, wk)
    c_wv = load(6, w_value, wv)
    c_k = load(7, keys, k_v)
    c_d = load(8, decay, d_v)
    c_v = load(9, values, v_v)
    c_fb = load(10, forget_bias, fb_v)
    c_og = load(11, out_gain, og_v)
    c_wo = load(12, w_out, wo.at[pl.ds(half, HD)])
    c_wg = load(13, w_gate, wg.at[pl.ds(0, FF_DEV)])
    c_wu = load(14, w_up, wu.at[pl.ds(0, FF_DEV)])
    c_wd = load(15, w_down, wd.at[pl.ds(0, FF_DEV)])

    tp_peers = []
    for dz in Z_ORDER:
        zz = lax.rem(z + (dz + 16), 16)
        for dc in (0, 1):
            cc = core if dc == 0 else 1 - core
            tp_peers.append(zz * 2 + cc)
    tp_peers.append(z * 2 + (1 - core))
    kv_peers = []
    for dist in (4, 3, 2, 1):
        for dy in (2, 1, 3, 0):
            for dx in (2, 1, 3, 0):
                if min(dy, 4 - dy) + min(dx, 4 - dx) == dist:
                    kv_peers.append(lax.rem(y + dy, 4) * 4 + lax.rem(x + dx, 4))

    barrier = pltpu.get_barrier_semaphore()
    for p in tp_peers:
        pl.semaphore_signal(barrier, inc=1, device_id={"tp": p}, device_id_type=MESH)
    for p in kv_peers:
        pl.semaphore_signal(barrier, inc=1, device_id={"kv": p}, device_id_type=MESH)

    def send(n, axis, peers, src, dst):
        for p in peers:
            pltpu.make_async_remote_copy(
                src_ref=src(p), dst_ref=dst, send_sem=ssem.at[n], recv_sem=rsem.at[n],
                device_id={axis: p}, device_id_type=MESH,
            ).start()

    def arrived(n, ref):
        pltpu.make_async_copy(ref, ref, rsem.at[n]).wait()

    def sent(n, ref):
        pltpu.make_async_copy(ref, ref, ssem.at[n]).wait()

    lane8 = iota((8, 128), 1)
    row8 = iota((8, 128), 0)
    lane1 = iota((1, 128), 1)
    ghalf8 = (lane8 // HD) == g
    mlane = (1 - g) * HD

    c_tok.wait()
    c_ag.wait()
    c_mg.wait()
    tok = tok_v[...].astype(F32)
    scaled = (tok * ag_v[...]).astype(BF16).astype(F32)
    row = jnp.concatenate(
        [scaled[0:1], scaled[1:2], scaled[2:3], tok[0:1], tok[1:2], tok[2:3], mg_v[...],
         jnp.zeros((1, 72), F32)], axis=1)
    buf1[pl.ds(tp, 1)] = row.reshape(1, 1, 128)

    wqf[pl.ds(other + 32, 32)] = jnp.zeros((32, 256), BF16)
    wo[pl.ds(other, HD)] = jnp.zeros((HD, 256), BF16)
    for w in (wg, wu, wd):
        w[FF_DEV:] = jnp.zeros((FF_PAD - FF_DEV, 256), BF16)
    c_wk.wait()
    c_wv.wait()
    wkv[...] = jnp.where(
        (iota((256, 128), 1) // HD) == g,
        wk[...].astype(F32), pltpu.roll(wv[...].astype(F32), HD, 1)).astype(BF16)
    c_wq.wait()
    c_wf.wait()

    pl.semaphore_wait(barrier, len(tp_peers) + len(kv_peers))
    send(0, "tp", tp_peers, lambda p: buf1.at[tp], buf1.at[tp])
    r24 = iota((24, 128), 0)
    b24 = r24 % 4
    want24 = jnp.where(
        r24 < 16,
        jnp.where((r24 < 4) | ((r24 >= 12) & (r24 < 16)), b24, -1),
        b24 + 3)
    l24 = iota((24, 128), 1)
    sel = jnp.where((b24 < 3) & (l24 // 8 == want24), 1.0, 0.0).astype(BF16)
    spread = (iota((256, 128), 0) % 8) == (iota((256, 128), 1) % 8)
    arrived(0, buf1.at[pl.ds(0, NTP - 1)])
    block = jnp.broadcast_to(buf1[...], (NTP, 8, 128)).reshape(256, 128)
    block = jnp.where(spread, block, 0.0)
    rows = dot(sel, block.astype(BF16), NT)
    tok_rows = rows[16:24]
    part = dot(rows[0:8].astype(BF16), wqf[...], NT) + dot(rows[8:16].astype(BF16), wkv[...], NN)
    squares = jnp.sum(tok_rows * tok_rows, axis=1, keepdims=True)
    part = jnp.where((lane8 == mlane + 32) & (row8 < 4), squares, part)
    buf2[pl.ds(kv, 1)] = part.reshape(1, 8, 128)
    send(1, "kv", kv_peers, lambda p: buf2.at[kv], buf2.at[kv])

    tok8 = jnp.where(row8 < 4, tok_rows[:, :128], tok_rows[:, 128:])
    gsel = jnp.where(lane8 // 8 == 6, 1.0, 0.0)
    gain_rows = dot(gsel, block, NT, precision=lax.Precision.HIGHEST)
    gain8 = jnp.where(row8 < 4, gain_rows[:, :128], gain_rows[:, 128:])
    c_fb.wait()
    c_og.wait()
    bias_row = jnp.concatenate([fb_v[...], jnp.zeros((1, 96), F32)], axis=1)
    bias = jnp.sum(jnp.where(lane1 == tp, bias_row, 0.0), axis=1, keepdims=True)
    og = og_v[pl.ds(z, 1)]
    og = jnp.where(core == g, og, pltpu.roll(og, HD, 1))

    arrived(1, buf2.at[pl.ds(0, NKV - 1)])
    total8 = jnp.sum(buf2[...], axis=0)
    sq = jnp.sum(jnp.where(lane8 == mlane + 32, total8, 0.0), axis=1, keepdims=True)
    rms1 = lax.rsqrt(sq * (1.0 / D) + EPS)
    q8 = jnp.where(ghalf8 & (row8 < 3), (total8 * rms1).astype(BF16).astype(F32), 0.0)
    for b in range(3):
        buf3[b, pl.ds(tp, 1)] = q8[b:b + 1].reshape(1, 1, 128)
    send(2, "tp", tp_peers, lambda p: buf3.at[:, tp], buf3.at[:, tp])

    kv8 = (pltpu.roll(total8, 4, 0) * rms1).astype(BF16).astype(F32)
    own = jnp.sum(q8 * kv8, axis=1, keepdims=True) * (HD ** -0.5)
    v8 = pltpu.roll(kv8, HD, 1)
    fj = jnp.sum(jnp.where(lane8 == mlane + tp, total8, 0.0), axis=1, keepdims=True) * rms1 + bias
    log_gate = jnp.minimum(fj, 0.0) - jnp.log1p(jnp.exp(-jnp.abs(fj)))
    c_k.wait()
    c_d.wait()
    c_v.wait()
    positions = (kv * NTP + tp) * SPAN + iota((32, SPAN), 1)
    lane32 = iota((32, 128), 1)
    ghalf32 = (lane32 // HD) == (iota((32, 128), 0) // 16)
    mlane32 = (1 - iota((32, 128), 0) // 16) * HD

    arrived(2, buf3.at[:, pl.ds(0, NTP - 1)])
    for b in range(3):
        qb = buf3[b].reshape(32, 128).astype(BF16)
        s = dot(qb, k_v[b], NN) * (HD ** -0.5) + d_v[b]
        live = positions < lengths[b]
        s = jnp.where(live, s, MASKED)
        top = jnp.max(s, axis=1, keepdims=True)
        w = jnp.where(live, jnp.exp(s - top), 0.0)
        tot = jnp.sum(w, axis=1, keepdims=True)
        vs = dot(w.astype(BF16), v_v[b], NT)
        msg = jnp.where(ghalf32, vs, jnp.where(lane32 == mlane32, top, tot))
        stage4[b] = msg.reshape(32, 1, 128)
    buf4[:, pl.ds(tp, 1)] = stage4[:, pl.ds(tp, 1)]
    send(3, "tp", tp_peers, lambda p: stage4.at[:, p], buf4.at[:, tp])

    def merge(y2):
        n = y2.shape[0]
        at_m = iota((n, 128), 1) == mlane
        m = jnp.sum(jnp.where(at_m, y2, 0.0), axis=1, keepdims=True)
        top2 = jnp.max(m, axis=0, keepdims=True)
        zsum = jnp.sum(jnp.exp(m - top2) * y2, axis=0, keepdims=True)
        return jnp.where(lane1 == mlane, top2, zsum)

    c_wo.wait()
    arrived(3, buf4.at[:, pl.ds(0, NTP - 1)])
    for b in range(3):
        buf5[b, pl.ds(kv, 1)] = merge(buf4[b].reshape(NTP, 128)).reshape(1, 1, 128)
    send(4, "kv", kv_peers, lambda p: buf5.at[:, kv], buf5.at[:, kv])
    arrived(4, buf5.at[:, pl.ds(0, NKV - 1)])
    zrow = jnp.concatenate(
        [merge(buf5[b].reshape(NKV, 128)) for b in range(3)] + [jnp.ones((5, 128), F32)], axis=0)
    m8 = jnp.sum(jnp.where(lane8 == mlane, zrow, 0.0), axis=1, keepdims=True) + log_gate
    l8 = jnp.sum(jnp.where(lane8 == mlane + 1, zrow, 0.0), axis=1, keepdims=True)
    top8 = jnp.maximum(m8, own)
    a8 = jnp.exp(m8 - top8)
    o8 = jnp.exp(own - top8)
    heads = (zrow * a8 + o8 * v8) / (l8 * a8 + o8)
    heads = jnp.where(ghalf8 & (row8 < 3), heads, 0.0)
    mean = jnp.sum(heads * heads, axis=1, keepdims=True) * (1.0 / HD)
    normed = heads * lax.rsqrt(mean + EPS) * og
    n_lo = normed.astype(BF16)
    n_hi = pltpu.roll(normed, 4, 0).astype(BF16)
    attn = dot(n_lo, wo[:, :128], NN) + dot(n_hi, wo[:, 128:], NN)
    buf6[pl.ds(tp, 1)] = attn.astype(BF16).reshape(1, 8, 128)
    send(5, "tp", tp_peers, lambda p: buf6.at[tp], buf6.at[tp])
    c_wg.wait()
    c_wu.wait()
    c_wd.wait()
    arrived(5, buf6.at[pl.ds(0, NTP - 1)])
    attn8 = jnp.sum(buf6[...].astype(F32), axis=0)
    res8 = (tok8 + attn8).astype(BF16).astype(F32)
    sc8 = (res8 * gain8).astype(BF16).astype(F32)
    sw8 = pltpu.roll(sc8, 4, 0)
    low = row8 < 4
    lhs_g = jnp.concatenate([jnp.where(low, sc8, 0.0), jnp.where(low, sw8, 0.0)], axis=1).astype(BF16)
    lhs_u = jnp.concatenate([jnp.where(low, 0.0, sw8), jnp.where(low, 0.0, sc8)], axis=1).astype(BF16)
    gu = dot(lhs_g, wg[...], NT) + dot(lhs_u, wu[...], NT)
    sq2 = jnp.sum(res8 * res8, axis=1, keepdims=True) + jnp.zeros((8, 128), F32)
    sq2 = sq2 + pltpu.roll(sq2, 4, 0)
    sq2_hi = sq2.astype(BF16).astype(F32)
    lane_t = lane8 + 256
    tail = jnp.where(lane_t == FF_DEV, sq2_hi, jnp.where(lane_t == FF_DEV + 1, sq2 - sq2_hi, gu[:, 256:]))
    gu = jnp.concatenate([gu[:, :256], tail], axis=1)
    buf7[pl.ds(kv, 1)] = gu.astype(BF16).reshape(1, 8, FF_PAD)
    send(6, "kv", kv_peers, lambda p: buf7.at[kv], buf7.at[kv])

    i64 = iota((64, 256), 0)
    n64 = iota((64, 256), 1)
    res_rows = jnp.concatenate([res8, pltpu.roll(res8, 4, 0)], axis=1)
    rep = jnp.broadcast_to(res_rows.reshape(8, 1, 256), (8, 8, 256)).reshape(64, 256)
    diag = (i64 % 8) == (n64 % 8)
    mine = jnp.where(iota((8, 256), 1) // 8 == tp, 1.0, 0.0).astype(BF16)
    res_mine = dot(mine, jnp.where(diag, rep, 0.0).astype(BF16), NT)[0:1]
    fold = jnp.where(iota((32, 256), 1) // 8 == iota((32, 256), 0), 1.0, 0.0).astype(BF16)

    arrived(6, buf7.at[pl.ds(0, NKV - 1)])
    gs = jnp.sum(buf7[...].astype(F32), axis=0)
    tail = gs[:, 256:]
    sq2 = jnp.sum(
        jnp.where((lane_t == FF_DEV) | (lane_t == FF_DEV + 1), tail, 0.0), axis=1, keepdims=True)
    rms2 = lax.rsqrt(sq2 * (1.0 / D) + EPS)
    gs = gs * jnp.concatenate([rms2[0:4], rms2[0:4]], axis=0)
    up = pltpu.roll(gs, 4, 0)
    hid = gs / (1.0 + jnp.exp(-gs)) * up
    hid = jnp.where((iota((8, FF_PAD), 1) < FF_DEV) & (iota((8, FF_PAD), 0) < 3), hid, 0.0)
    hid = jnp.broadcast_to(hid.reshape(8, 1, FF_PAD), (8, 8, FF_PAD)).reshape(64, FF_PAD)
    down = dot(hid.astype(BF16), wd[...], NN)
    down = jnp.where(diag, down, 0.0)
    d_hi = down.astype(BF16)
    d_lo = (down - d_hi.astype(F32)).astype(BF16)
    parts = dot(fold, d_hi, NT) + dot(fold, d_lo, NT)
    parts = jnp.concatenate([parts, jnp.zeros((32, 64), F32)], axis=1)
    stage8[...] = parts.reshape(32, 1, 128)
    buf8[pl.ds(tp, 1)] = stage8[pl.ds(tp, 1)]
    send(7, "tp", tp_peers, lambda p: stage8.at[p], buf8.at[tp])
    arrived(7, buf8.at[pl.ds(0, NTP - 1)])
    share = jnp.sum(buf8[...], axis=0)[:, :64] + res_mine
    out[...] = jnp.concatenate([share[:, 0:8], share[:, 8:16], share[:, 16:24]], axis=0).astype(BF16)

    sent(0, buf1.at[pl.ds(0, NTP - 1)])
    sent(1, buf2.at[pl.ds(0, NKV - 1)])
    sent(2, buf3.at[:, pl.ds(0, NTP - 1)])
    sent(3, buf4.at[:, pl.ds(0, NTP - 1)])
    sent(4, buf5.at[:, pl.ds(0, NKV - 1)])
    sent(5, buf6.at[pl.ds(0, NTP - 1)])
    sent(6, buf7.at[pl.ds(0, NKV - 1)])
    sent(7, buf8.at[pl.ds(0, NTP - 1)])


def body(
    tokens, lengths, attn_gain, w_query, w_key, w_value, w_forget, forget_bias,
    cache_keys, cache_values, cache_decay, out_gain, w_out, mlp_gain, w_gate, w_up, w_down,
):
    hbm = pl.BlockSpec(memory_space=pl.ANY)
    v = pltpu.VMEM
    return pl.pallas_call(
        kernel,
        out_shape=jax.ShapeDtypeStruct((3, 8), BF16),
        in_specs=[pl.BlockSpec(memory_space=pltpu.SMEM)] + [hbm] * 16,
        out_specs=pl.BlockSpec(memory_space=pltpu.VMEM),
        scratch_shapes=[
            v((3, 8), BF16), v((1, 8), F32), v((1, 8), F32), v((1, 32), F32), v((16, 128), F32),
            v((128, 256), BF16), v((256, 128), BF16), v((256, 128), BF16), v((256, 128), BF16),
            v((3, 128, SPAN), BF16), v((3, 128, SPAN), BF16), v((3, 32, SPAN), F32),
            v((128, 256), BF16),
            v((FF_PAD, 256), BF16), v((FF_PAD, 256), BF16), v((FF_PAD, 256), BF16),
            v((NTP, 1, 128), F32), v((NKV, 8, 128), F32), v((3, NTP, 1, 128), F32),
            v((3, NTP, 1, 128), F32), v((3, NTP, 1, 128), F32), v((3, NKV, 1, 128), F32),
            v((NTP, 8, 128), BF16), v((NKV, 8, FF_PAD), BF16),
            v((NTP, 1, 128), F32), v((NTP, 1, 128), F32),
            pltpu.SemaphoreType.DMA((16,)),
            pltpu.SemaphoreType.DMA((8,)),
            pltpu.SemaphoreType.DMA((8,)),
        ],
        compiler_params=pltpu.CompilerParams(
            collective_id=0, has_side_effects=True, vmem_limit_bytes=60 * 1024 * 1024),
    )(
        lengths, tokens, attn_gain.reshape(1, 8), mlp_gain.reshape(1, 8),
        forget_bias.reshape(1, 32), out_gain.reshape(16, 128),
        w_query.T, w_key, w_value, w_forget.T, cache_keys, cache_values, cache_decay, w_out,
        w_gate.T, w_up.T, w_down,
    )


def solution(mesh):
    kvtp = ("kv", "tp")
    placed = (
        P(None, kvtp), P(), P(kvtp), P("kv", "tp"), P("kv", None), P("kv", None), P(), P(),
        P(None, None, kvtp), P(None, None, kvtp), P(None, None, kvtp), P(), P("tp", "kv"),
        P(kvtp), P("kv", "tp"), P("kv", "tp"), P("tp", "kv"),
    )
    return jax.shard_map(
        body, mesh=mesh, in_specs=placed, out_specs=P(None, kvtp), check_vma=False)
```

time: 253 us -> 71.2 us (0.28)
  blocking collectives: 137 us -> 0 us
  Pallas kernels: 0 us -> 69.8 us
  waiting for transfers between devices: 58.1 us -> 0 us
  starting transfers between devices: 39.5 us -> 0 us
  local copies, waits for them, and re-layouts: 13.8 us -> 1.24 us
    pallas_call x0 -> x1, Pallas kernels: none -> 69.8 us  [body(): pl.pallas_call(kernel, out_shape=jax.ShapeDtypeStruct((3, 8), BF16), in_s...]
    all_to_all x5 -> x0, waiting for transfers between devices: 58.1 us -> none  [sent_to_all(): return lax.all_to_all(copies, axis, split_axis=0, concat_axis=0, tiled=True)]
    all_gather x4 -> x0, blocking collectives: 56.1 us -> none  [all_in_one(): both, at, found = (lax.all_gather(jnp.concatenate(lines), axis), 0, {})]
    all_to_all x2 -> x0, blocking collectives: 41.1 us -> none  [summed_on_arrival(): blocks = lax.all_to_all(in_blocks(x, dim, length), axis, 0, 0, tiled=True)]
    psum x4 -> x0, blocking collectives: 39.6 us -> none  [by_axis(): x = lax.psum(x, axis)]
    all_to_all x5 -> x0, starting transfers between devices: 39.5 us -> none  [sent_to_all(): return lax.all_to_all(copies, axis, split_axis=0, concat_axis=0, tiled=True)]
    broadcast_in_dim x6 -> x0, local copies, waits for them, and re-layouts: 3.05 us -> none  [the longest x5 3.04 us: sent_to_all(): copies = jnp.broadcast_to(x, (lax.axis_size(axis), *x.shape))]
    reshape x29 -> x0, local copies, waits for them, and re-layouts: 2.58 us -> none  [the longest x17 1.54 us: all_in_one(): jnp.pad(leaves[k].reshape(-1), (0, -leaves[k].size % width))]
  transfers between devices with their start and end apart: 5 -> 0, of which waited for: 5 -> 0; matrix products, arithmetic and copies ran while one was open for 1% -> 0% of each run, Pallas kernels for 0% -> 0%
where the time goes in v1:
time: 71.2 us; the launch traced here: 71 us
  Pallas kernels  69.8 us (98%)
  local copies, waits for them, and re-layouts  1.24 us (2%)
    pallas_call x1, Pallas kernels, body(): pl.pallas_call(kernel, out_shape=jax.ShapeDtypeStruct((3, 8), BF16), in_s...  69.8 us

profile of v1, /device:TPU:1, one launch (start us, length us, event | category | flops | bytes accessed | tf_op | source)
XLA Modules:
  0.0 71.0 jit_solution(11485056236989830094)
XLA Ops:
  0.0 69.8 %shard_map.163 = bf16[3,8]{1,0:T(4,128)(2,1)} custom-call(s32[3]{0:T(128)} %lengths.1, bf16[3,8]{1,0:T(4,128)(2,1)} %tokens.1, f32[1,8]{1,0:T(1,128)} %bitcast.13, f32[1,8]{1,0:T(1,128)} %bitcast.14, f32[1,32]{1,0:T(1,128)} %bitcast.15, f32[16,128]{1,0:T(8,128)} %bitcast.12, bf16[64,256]{1,0:T(8,128)(2,1)} %bitcast.11, bf16[256,128]{1,0:T(8,128)(2,1)} %w_key.1, ...), custom_call_target="tpu_custom_call" | custom-call | tf_op jit(solution)/shard_map/pallas_call | solution.py:309
  69.8 1.2 %copy.19 = bf16[3,8]{1,0:T(4,128)(2,1)} copy(bf16[3,8]{1,0:T(4,128)(2,1)} %shard_map.163) | data formatting | bytes 96

commit v2 on v1

--- a/solution.py
+++ b/solution.py
@@ -308,7 +308,7 @@
     v = pltpu.VMEM
     return pl.pallas_call(
         kernel,
-        out_shape=jax.ShapeDtypeStruct((3, 8), BF16),
+        out_shape=pltpu.VMEM((3, 8), BF16),
         in_specs=[pl.BlockSpec(memory_space=pltpu.SMEM)] + [hbm] * 16,
         out_specs=pl.BlockSpec(memory_space=pltpu.VMEM),
         scratch_shapes=[

time: 71.2 us -> 69.9 us (0.982)
  no operation moved by 1% of the time
where the time goes in v2:
time: 69.9 us; the launch traced here: 69.8 us
  Pallas kernels  69.2 us (99%)
    pallas_call x1, Pallas kernels, body(): pl.pallas_call(kernel, out_shape=pltpu.VMEM((3, 8), BF16), in_specs=[pl.B...  69.2 us

profile of v2, /device:TPU:1, one launch (start us, length us, event | category | flops | bytes accessed | tf_op | source)
XLA Modules:
  0.0 69.8 jit_solution(17455605403218449337)
XLA Ops:
  0.0 69.2 %shard_map.163 = bf16[3,8]{1,0:T(4,128)(2,1)S(1)} custom-call(s32[3]{0:T(128)} %lengths.1, bf16[3,8]{1,0:T(4,128)(2,1)} %tokens.1, f32[1,8]{1,0:T(1,128)} %bitcast.13, f32[1,8]{1,0:T(1,128)} %bitcast.14, f32[1,32]{1,0:T(1,128)} %bitcast.15, f32[16,128]{1,0:T(8,128)} %bitcast.12, bf16[64,256]{1,0:T(8,128)(2,1)} %bitcast.11, bf16[256,128]{1,0:T(8,128)(2,1)} %w_key.1, ...), custom_call_target="tpu_custom_call" | custom-call | tf_op jit(solution)/shard_map/pallas_call | solution.py:309
  69.2 0.6 copy.19

commit v3 on v2

--- a/solution.py
+++ b/solution.py
@@ -21,9 +21,6 @@
 NT = (((1,), (1,)), ((), ()))
 NN = (((1,), (0,)), ((), ()))
 
-Z_ORDER = [8, 7, -7, 6, -6, 5, -5, 4, -4, 3, -3, 2, -2, 1, -1]
-
-
 def dot(a, b, dims, **kw):
     return lax.dot_general(a, b, dims, preferred_element_type=F32, **kw)
 
@@ -33,11 +30,11 @@
 
 
 def kernel(
-    lengths, tokens, attn_gain, mlp_gain, forget_bias, out_gain,
+    lengths_h, tokens, attn_gain, mlp_gain, forget_bias, out_gain,
     w_query, w_key, w_value, w_forget, keys, values, decay, w_out,
     w_gate, w_up, w_down,
     out,
-    tok_v, ag_v, mg_v, fb_v, og_v, wqf, wk, wv, wkv, k_v, v_v, d_v, wo,
+    lengths, tok_v, ag_v, mg_v, fb_v, og_v, wqf, wk, wv, wkv, k_v, v_v, d_v, wo,
     wg, wu, wd,
     buf1, buf2, buf3, stage4, buf4, buf5, buf6, buf7, stage8, buf8,
     lsem, ssem, rsem,
@@ -49,6 +46,29 @@
     core = tp % 2
     y = kv // 4
     x = kv % 4
+
+    kv_peers = []
+    for dist in (4, 3, 2, 1):
+        for dy in (2, 1, 3, 0):
+            for dx in (2, 1, 3, 0):
+                if min(dy, 4 - dy) + min(dx, 4 - dx) == dist:
+                    kv_peers.append(lax.rem(y + dy, 4) * 4 + lax.rem(x + dx, 4))
+
+    barrier = pltpu.get_barrier_semaphore()
+
+    def far_peer(i):
+        s = i // 2
+        d = 8 - (s + 1) // 2
+        return lax.rem(z + d + (16 - 2 * d) * (1 - s % 2), 16) * 2 + lax.rem(core + i, 2)
+
+    def greet(i, carry):
+        pl.semaphore_signal(barrier, inc=1, device_id={"tp": far_peer(i)}, device_id_type=MESH)
+        return carry
+    lax.fori_loop(0, 30, greet, 0)
+    partner = z * 2 + (1 - core)
+    pl.semaphore_signal(barrier, inc=1, device_id={"tp": partner}, device_id_type=MESH)
+    for p in kv_peers:
+        pl.semaphore_signal(barrier, inc=1, device_id={"kv": p}, device_id_type=MESH)
 
     def load(i, src, dst):
         c = pltpu.make_async_copy(src, dst, lsem.at[i])
@@ -74,33 +94,24 @@
     c_wg = load(13, w_gate, wg.at[pl.ds(0, FF_DEV)])
     c_wu = load(14, w_up, wu.at[pl.ds(0, FF_DEV)])
     c_wd = load(15, w_down, wd.at[pl.ds(0, FF_DEV)])
-
-    tp_peers = []
-    for dz in Z_ORDER:
-        zz = lax.rem(z + (dz + 16), 16)
-        for dc in (0, 1):
-            cc = core if dc == 0 else 1 - core
-            tp_peers.append(zz * 2 + cc)
-    tp_peers.append(z * 2 + (1 - core))
-    kv_peers = []
-    for dist in (4, 3, 2, 1):
-        for dy in (2, 1, 3, 0):
-            for dx in (2, 1, 3, 0):
-                if min(dy, 4 - dy) + min(dx, 4 - dx) == dist:
-                    kv_peers.append(lax.rem(y + dy, 4) * 4 + lax.rem(x + dx, 4))
-
-    barrier = pltpu.get_barrier_semaphore()
-    for p in tp_peers:
-        pl.semaphore_signal(barrier, inc=1, device_id={"tp": p}, device_id_type=MESH)
-    for p in kv_peers:
-        pl.semaphore_signal(barrier, inc=1, device_id={"kv": p}, device_id_type=MESH)
+    c_len = load(16, lengths_h, lengths)
 
     def send(n, axis, peers, src, dst):
-        for p in peers:
+        def one(p):
             pltpu.make_async_remote_copy(
                 src_ref=src(p), dst_ref=dst, send_sem=ssem.at[n], recv_sem=rsem.at[n],
                 device_id={axis: p}, device_id_type=MESH,
             ).start()
+        if axis == "kv":
+            for p in peers:
+                one(p)
+            return
+
+        def step(i, carry):
+            one(far_peer(i))
+            return carry
+        lax.fori_loop(0, 30, step, 0)
+        one(partner)
 
     def arrived(n, ref):
         pltpu.make_async_copy(ref, ref, rsem.at[n]).wait()
@@ -136,8 +147,8 @@
     c_wq.wait()
     c_wf.wait()
 
-    pl.semaphore_wait(barrier, len(tp_peers) + len(kv_peers))
-    send(0, "tp", tp_peers, lambda p: buf1.at[tp], buf1.at[tp])
+    pl.semaphore_wait(barrier, NTP - 1 + len(kv_peers))
+    send(0, "tp", (), lambda p: buf1.at[tp], buf1.at[tp])
     r24 = iota((24, 128), 0)
     b24 = r24 % 4
     want24 = jnp.where(
@@ -169,6 +180,7 @@
     og = og_v[pl.ds(z, 1)]
     og = jnp.where(core == g, og, pltpu.roll(og, HD, 1))
 
+    sent(0, buf1.at[pl.ds(0, NTP - 1)])
     arrived(1, buf2.at[pl.ds(0, NKV - 1)])
     total8 = jnp.sum(buf2[...], axis=0)
     sq = jnp.sum(jnp.where(lane8 == mlane + 32, total8, 0.0), axis=1, keepdims=True)
@@ -176,7 +188,7 @@
     q8 = jnp.where(ghalf8 & (row8 < 3), (total8 * rms1).astype(BF16).astype(F32), 0.0)
     for b in range(3):
         buf3[b, pl.ds(tp, 1)] = q8[b:b + 1].reshape(1, 1, 128)
-    send(2, "tp", tp_peers, lambda p: buf3.at[:, tp], buf3.at[:, tp])
+    send(2, "tp", (), lambda p: buf3.at[:, tp], buf3.at[:, tp])
 
     kv8 = (pltpu.roll(total8, 4, 0) * rms1).astype(BF16).astype(F32)
     own = jnp.sum(q8 * kv8, axis=1, keepdims=True) * (HD ** -0.5)
@@ -186,11 +198,13 @@
     c_k.wait()
     c_d.wait()
     c_v.wait()
+    c_len.wait()
     positions = (kv * NTP + tp) * SPAN + iota((32, SPAN), 1)
     lane32 = iota((32, 128), 1)
     ghalf32 = (lane32 // HD) == (iota((32, 128), 0) // 16)
     mlane32 = (1 - iota((32, 128), 0) // 16) * HD
 
+    sent(1, buf2.at[pl.ds(0, NKV - 1)])
     arrived(2, buf3.at[:, pl.ds(0, NTP - 1)])
     for b in range(3):
         qb = buf3[b].reshape(32, 128).astype(BF16)
@@ -204,7 +218,7 @@
         msg = jnp.where(ghalf32, vs, jnp.where(lane32 == mlane32, top, tot))
         stage4[b] = msg.reshape(32, 1, 128)
     buf4[:, pl.ds(tp, 1)] = stage4[:, pl.ds(tp, 1)]
-    send(3, "tp", tp_peers, lambda p: stage4.at[:, p], buf4.at[:, tp])
+    send(3, "tp", (), lambda p: stage4.at[:, p], buf4.at[:, tp])
 
     def merge(y2):
         n = y2.shape[0]
@@ -215,10 +229,12 @@
         return jnp.where(lane1 == mlane, top2, zsum)
 
     c_wo.wait()
+    sent(2, buf3.at[:, pl.ds(0, NTP - 1)])
     arrived(3, buf4.at[:, pl.ds(0, NTP - 1)])
     for b in range(3):
         buf5[b, pl.ds(kv, 1)] = merge(buf4[b].reshape(NTP, 128)).reshape(1, 1, 128)
     send(4, "kv", kv_peers, lambda p: buf5.at[:, kv], buf5.at[:, kv])
+    sent(3, buf4.at[:, pl.ds(0, NTP - 1)])
     arrived(4, buf5.at[:, pl.ds(0, NKV - 1)])
     zrow = jnp.concatenate(
         [merge(buf5[b].reshape(NKV, 128)) for b in range(3)] + [jnp.ones((5, 128), F32)], axis=0)
@@ -235,10 +251,11 @@
     n_hi = pltpu.roll(normed, 4, 0).astype(BF16)
     attn = dot(n_lo, wo[:, :128], NN) + dot(n_hi, wo[:, 128:], NN)
     buf6[pl.ds(tp, 1)] = attn.astype(BF16).reshape(1, 8, 128)
-    send(5, "tp", tp_peers, lambda p: buf6.at[tp], buf6.at[tp])
+    send(5, "tp", (), lambda p: buf6.at[tp], buf6.at[tp])
     c_wg.wait()
     c_wu.wait()
     c_wd.wait()
+    sent(4, buf5.at[:, pl.ds(0, NKV - 1)])
     arrived(5, buf6.at[pl.ds(0, NTP - 1)])
     attn8 = jnp.sum(buf6[...].astype(F32), axis=0)
     res8 = (tok8 + attn8).astype(BF16).astype(F32)
@@ -266,6 +283,7 @@
     res_mine = dot(mine, jnp.where(diag, rep, 0.0).astype(BF16), NT)[0:1]
     fold = jnp.where(iota((32, 256), 1) // 8 == iota((32, 256), 0), 1.0, 0.0).astype(BF16)
 
+    sent(5, buf6.at[pl.ds(0, NTP - 1)])
     arrived(6, buf7.at[pl.ds(0, NKV - 1)])
     gs = jnp.sum(buf7[...].astype(F32), axis=0)
     tail = gs[:, 256:]
@@ -285,18 +303,11 @@
     parts = jnp.concatenate([parts, jnp.zeros((32, 64), F32)], axis=1)
     stage8[...] = parts.reshape(32, 1, 128)
     buf8[pl.ds(tp, 1)] = stage8[pl.ds(tp, 1)]
-    send(7, "tp", tp_peers, lambda p: stage8.at[p], buf8.at[tp])
+    send(7, "tp", (), lambda p: stage8.at[p], buf8.at[tp])
+    sent(6, buf7.at[pl.ds(0, NKV - 1)])
     arrived(7, buf8.at[pl.ds(0, NTP - 1)])
     share = jnp.sum(buf8[...], axis=0)[:, :64] + res_mine
     out[...] = jnp.concatenate([share[:, 0:8], share[:, 8:16], share[:, 16:24]], axis=0).astype(BF16)
-
-    sent(0, buf1.at[pl.ds(0, NTP - 1)])
-    sent(1, buf2.at[pl.ds(0, NKV - 1)])
-    sent(2, buf3.at[:, pl.ds(0, NTP - 1)])
-    sent(3, buf4.at[:, pl.ds(0, NTP - 1)])
-    sent(4, buf5.at[:, pl.ds(0, NKV - 1)])
-    sent(5, buf6.at[pl.ds(0, NTP - 1)])
-    sent(6, buf7.at[pl.ds(0, NKV - 1)])
     sent(7, buf8.at[pl.ds(0, NTP - 1)])
 
 
@@ -309,10 +320,10 @@
     return pl.pallas_call(
         kernel,
         out_shape=pltpu.VMEM((3, 8), BF16),
-        in_specs=[pl.BlockSpec(memory_space=pltpu.SMEM)] + [hbm] * 16,
+        in_specs=[hbm] * 17,
         out_specs=pl.BlockSpec(memory_space=pltpu.VMEM),
         scratch_shapes=[
-            v((3, 8), BF16), v((1, 8), F32), v((1, 8), F32), v((1, 32), F32), v((16, 128), F32),
+            pltpu.SMEM((3,), jnp.int32), v((3, 8), BF16), v((1, 8), F32), v((1, 8), F32), v((1, 32), F32), v((16, 128), F32),
             v((128, 256), BF16), v((256, 128), BF16), v((256, 128), BF16), v((256, 128), BF16),
             v((3, 128, SPAN), BF16), v((3, 128, SPAN), BF16), v((3, 32, SPAN), F32),
             v((128, 256), BF16),
@@ -321,7 +332,7 @@
             v((3, NTP, 1, 128), F32), v((3, NTP, 1, 128), F32), v((3, NKV, 1, 128), F32),
             v((NTP, 8, 128), BF16), v((NKV, 8, FF_PAD), BF16),
             v((NTP, 1, 128), F32), v((NTP, 1, 128), F32),
-            pltpu.SemaphoreType.DMA((16,)),
+            pltpu.SemaphoreType.DMA((17,)),
             pltpu.SemaphoreType.DMA((8,)),
             pltpu.SemaphoreType.DMA((8,)),
         ],

time: 69.9 us -> 69 us (0.987)
  Pallas kernels: 69.2 us -> 68.3 us
    pallas_call x1, Pallas kernels: 69.2 us -> 68.3 us  [body(): pl.pallas_call(kernel, out_shape=pltpu.VMEM((3, 8), BF16), in_specs=[hbm]...]
where the time goes in v3:
time: 69 us; the launch traced here: 68.9 us
  Pallas kernels  68.3 us (99%)
    pallas_call x1, Pallas kernels, body(): pl.pallas_call(kernel, out_shape=pltpu.VMEM((3, 8), BF16), in_specs=[hbm]...  68.3 us

profile of v3, /device:TPU:1, one launch (start us, length us, event | category | flops | bytes accessed | tf_op | source)
XLA Modules:
  0.0 68.9 jit_solution(14023818107594685612)
XLA Ops:
  0.0 68.3 %shard_map.163 = bf16[3,8]{1,0:T(4,128)(2,1)S(1)} custom-call(s32[3]{0:T(128)} %lengths_h.1, bf16[3,8]{1,0:T(4,128)(2,1)} %tokens.1, f32[1,8]{1,0:T(1,128)} %bitcast.13, f32[1,8]{1,0:T(1,128)} %bitcast.14, f32[1,32]{1,0:T(1,128)} %bitcast.15, f32[16,128]{1,0:T(8,128)} %bitcast.12, bf16[64,256]{1,0:T(8,128)(2,1)} %bitcast.11, bf16[256,128]{1,0:T(8,128)(2,1)} %w_key.1, ...), custom_call_target="tpu_custom_call" | custom-call | tf_op jit(solution)/shard_map/pallas_call | solution.py:320
  68.4 0.6 copy.19

commit v4 on v3

--- a/solution.py
+++ b/solution.py
@@ -37,7 +37,7 @@
     lengths, tok_v, ag_v, mg_v, fb_v, og_v, wqf, wk, wv, wkv, k_v, v_v, d_v, wo,
     wg, wu, wd,
     buf1, buf2, buf3, stage4, buf4, buf5, buf6, buf7, stage8, buf8,
-    lsem, ssem, rsem,
+    lsem, ssem, rsem, pair_ready,
 ):
     kv = lax.axis_index("kv")
     tp = lax.axis_index("tp")
@@ -61,10 +61,10 @@
         d = 8 - (s + 1) // 2
         return lax.rem(z + d + (16 - 2 * d) * (1 - s % 2), 16) * 2 + lax.rem(core + i, 2)
 
-    def greet(i, carry):
-        pl.semaphore_signal(barrier, inc=1, device_id={"tp": far_peer(i)}, device_id_type=MESH)
+    def greet(s, carry):
+        pl.semaphore_signal(barrier, inc=1, device_id={"tp": far_peer(2 * s)}, device_id_type=MESH)
         return carry
-    lax.fori_loop(0, 30, greet, 0)
+    lax.fori_loop(0, 15, greet, 0)
     partner = z * 2 + (1 - core)
     pl.semaphore_signal(barrier, inc=1, device_id={"tp": partner}, device_id_type=MESH)
     for p in kv_peers:
@@ -147,8 +147,26 @@
     c_wq.wait()
     c_wf.wait()
 
-    pl.semaphore_wait(barrier, NTP - 1 + len(kv_peers))
-    send(0, "tp", (), lambda p: buf1.at[tp], buf1.at[tp])
+    pl.semaphore_wait(barrier, 16 + len(kv_peers))
+    pl.semaphore_signal(pair_ready, inc=1, device_id={"tp": partner}, device_id_type=MESH)
+
+    def token_copy(p):
+        pltpu.make_async_remote_copy(
+            src_ref=buf1.at[tp], dst_ref=buf1.at[tp], send_sem=ssem.at[0], recv_sem=rsem.at[0],
+            device_id={"tp": p}, device_id_type=MESH,
+        ).start()
+
+    def same_core(s, carry):
+        token_copy(far_peer(2 * s))
+        return carry
+
+    def other_core(s, carry):
+        token_copy(far_peer(2 * s + 1))
+        return carry
+    lax.fori_loop(0, 15, same_core, 0)
+    pl.semaphore_wait(pair_ready, 1)
+    lax.fori_loop(0, 15, other_core, 0)
+    token_copy(partner)
     r24 = iota((24, 128), 0)
     b24 = r24 % 4
     want24 = jnp.where(
@@ -187,8 +205,8 @@
     rms1 = lax.rsqrt(sq * (1.0 / D) + EPS)
     q8 = jnp.where(ghalf8 & (row8 < 3), (total8 * rms1).astype(BF16).astype(F32), 0.0)
     for b in range(3):
-        buf3[b, pl.ds(tp, 1)] = q8[b:b + 1].reshape(1, 1, 128)
-    send(2, "tp", (), lambda p: buf3.at[:, tp], buf3.at[:, tp])
+        buf3[b, pl.ds(tp, 1)] = q8[b:b + 1]
+    send(2, "tp", (), lambda p: buf3.at[:, pl.ds(tp, 1)], buf3.at[:, pl.ds(tp, 1)])
 
     kv8 = (pltpu.roll(total8, 4, 0) * rms1).astype(BF16).astype(F32)
     own = jnp.sum(q8 * kv8, axis=1, keepdims=True) * (HD ** -0.5)
@@ -207,7 +225,7 @@
     sent(1, buf2.at[pl.ds(0, NKV - 1)])
     arrived(2, buf3.at[:, pl.ds(0, NTP - 1)])
     for b in range(3):
-        qb = buf3[b].reshape(32, 128).astype(BF16)
+        qb = buf3[b].astype(BF16)
         s = dot(qb, k_v[b], NN) * (HD ** -0.5) + d_v[b]
         live = positions < lengths[b]
         s = jnp.where(live, s, MASKED)
@@ -216,9 +234,9 @@
         tot = jnp.sum(w, axis=1, keepdims=True)
         vs = dot(w.astype(BF16), v_v[b], NT)
         msg = jnp.where(ghalf32, vs, jnp.where(lane32 == mlane32, top, tot))
-        stage4[b] = msg.reshape(32, 1, 128)
+        stage4[b] = msg
     buf4[:, pl.ds(tp, 1)] = stage4[:, pl.ds(tp, 1)]
-    send(3, "tp", (), lambda p: stage4.at[:, p], buf4.at[:, tp])
+    send(3, "tp", (), lambda p: stage4.at[:, pl.ds(p, 1)], buf4.at[:, pl.ds(tp, 1)])
 
     def merge(y2):
         n = y2.shape[0]
@@ -232,12 +250,12 @@
     sent(2, buf3.at[:, pl.ds(0, NTP - 1)])
     arrived(3, buf4.at[:, pl.ds(0, NTP - 1)])
     for b in range(3):
-        buf5[b, pl.ds(kv, 1)] = merge(buf4[b].reshape(NTP, 128)).reshape(1, 1, 128)
-    send(4, "kv", kv_peers, lambda p: buf5.at[:, kv], buf5.at[:, kv])
+        buf5[b, pl.ds(kv, 1)] = merge(buf4[b])
+    send(4, "kv", kv_peers, lambda p: buf5.at[:, pl.ds(kv, 1)], buf5.at[:, pl.ds(kv, 1)])
     sent(3, buf4.at[:, pl.ds(0, NTP - 1)])
     arrived(4, buf5.at[:, pl.ds(0, NKV - 1)])
     zrow = jnp.concatenate(
-        [merge(buf5[b].reshape(NKV, 128)) for b in range(3)] + [jnp.ones((5, 128), F32)], axis=0)
+        [merge(buf5[b]) for b in range(3)] + [jnp.ones((5, 128), F32)], axis=0)
     m8 = jnp.sum(jnp.where(lane8 == mlane, zrow, 0.0), axis=1, keepdims=True) + log_gate
     l8 = jnp.sum(jnp.where(lane8 == mlane + 1, zrow, 0.0), axis=1, keepdims=True)
     top8 = jnp.maximum(m8, own)
@@ -328,13 +346,14 @@
             v((3, 128, SPAN), BF16), v((3, 128, SPAN), BF16), v((3, 32, SPAN), F32),
             v((128, 256), BF16),
             v((FF_PAD, 256), BF16), v((FF_PAD, 256), BF16), v((FF_PAD, 256), BF16),
-            v((NTP, 1, 128), F32), v((NKV, 8, 128), F32), v((3, NTP, 1, 128), F32),
-            v((3, NTP, 1, 128), F32), v((3, NTP, 1, 128), F32), v((3, NKV, 1, 128), F32),
+            v((NTP, 1, 128), F32), v((NKV, 8, 128), F32), v((3, NTP, 128), F32),
+            v((3, NTP, 128), F32), v((3, NTP, 128), F32), v((3, NKV, 128), F32),
             v((NTP, 8, 128), BF16), v((NKV, 8, FF_PAD), BF16),
             v((NTP, 1, 128), F32), v((NTP, 1, 128), F32),
             pltpu.SemaphoreType.DMA((17,)),
             pltpu.SemaphoreType.DMA((8,)),
             pltpu.SemaphoreType.DMA((8,)),
+            pltpu.SemaphoreType.REGULAR,
         ],
         compiler_params=pltpu.CompilerParams(
             collective_id=0, has_side_effects=True, vmem_limit_bytes=60 * 1024 * 1024),

time: 69 us -> 68.9 us (level)
  no operation moved by 1% of the time
where the time goes in v4:
time: 68.9 us; the launch traced here: 68.8 us
  Pallas kernels  68.2 us (99%)
    pallas_call x1, Pallas kernels, body(): pl.pallas_call(kernel, out_shape=pltpu.VMEM((3, 8), BF16), in_specs=[hbm]...  68.2 us

profile of v4, /device:TPU:1, one launch (start us, length us, event | category | flops | bytes accessed | tf_op | source)
XLA Modules:
  0.0 68.8 jit_solution(3555864807969221435)
XLA Ops:
  0.0 68.2 %shard_map.163 = bf16[3,8]{1,0:T(4,128)(2,1)S(1)} custom-call(s32[3]{0:T(128)} %lengths_h.1, bf16[3,8]{1,0:T(4,128)(2,1)} %tokens.1, f32[1,8]{1,0:T(1,128)} %bitcast.13, f32[1,8]{1,0:T(1,128)} %bitcast.14, f32[1,32]{1,0:T(1,128)} %bitcast.15, f32[16,128]{1,0:T(8,128)} %bitcast.12, bf16[64,256]{1,0:T(8,128)(2,1)} %bitcast.11, bf16[256,128]{1,0:T(8,128)(2,1)} %w_key.1, ...), custom_call_target="tpu_custom_call" | custom-call | tf_op jit(solution)/shard_map/pallas_call | solution.py:338
  68.2 0.6 copy.19

commit v5 on v4

--- a/solution.py
+++ b/solution.py
@@ -150,23 +150,8 @@
     pl.semaphore_wait(barrier, 16 + len(kv_peers))
     pl.semaphore_signal(pair_ready, inc=1, device_id={"tp": partner}, device_id_type=MESH)
 
-    def token_copy(p):
-        pltpu.make_async_remote_copy(
-            src_ref=buf1.at[tp], dst_ref=buf1.at[tp], send_sem=ssem.at[0], recv_sem=rsem.at[0],
-            device_id={"tp": p}, device_id_type=MESH,
-        ).start()
-
-    def same_core(s, carry):
-        token_copy(far_peer(2 * s))
-        return carry
-
-    def other_core(s, carry):
-        token_copy(far_peer(2 * s + 1))
-        return carry
-    lax.fori_loop(0, 15, same_core, 0)
     pl.semaphore_wait(pair_ready, 1)
-    lax.fori_loop(0, 15, other_core, 0)
-    token_copy(partner)
+    send(0, "tp", (), lambda p: buf1.at[tp], buf1.at[tp])
     r24 = iota((24, 128), 0)
     b24 = r24 % 4
     want24 = jnp.where(

time: 68.9 us -> 68.7 us (level)
  no operation moved by 1% of the time
where the time goes in v5:
time: 68.7 us; the launch traced here: 68.5 us
  Pallas kernels  68 us (99%)
    pallas_call x1, Pallas kernels, body(): pl.pallas_call(kernel, out_shape=pltpu.VMEM((3, 8), BF16), in_specs=[hbm]...  68 us

profile of v5, /device:TPU:1, one launch (start us, length us, event | category | flops | bytes accessed | tf_op | source)
XLA Modules:
  0.0 68.5 jit_solution(5603664336960606005)
XLA Ops:
  0.0 68.0 %shard_map.163 = bf16[3,8]{1,0:T(4,128)(2,1)S(1)} custom-call(s32[3]{0:T(128)} %lengths_h.1, bf16[3,8]{1,0:T(4,128)(2,1)} %tokens.1, f32[1,8]{1,0:T(1,128)} %bitcast.13, f32[1,8]{1,0:T(1,128)} %bitcast.14, f32[1,32]{1,0:T(1,128)} %bitcast.15, f32[16,128]{1,0:T(8,128)} %bitcast.12, bf16[64,256]{1,0:T(8,128)(2,1)} %bitcast.11, bf16[256,128]{1,0:T(8,128)(2,1)} %w_key.1, ...), custom_call_target="tpu_custom_call" | custom-call | tf_op jit(solution)/shard_map/pallas_call | solution.py:323
  68.0 0.6 copy.19

commit v6 on v5

--- a/solution.py
+++ b/solution.py
@@ -208,20 +208,20 @@
     mlane32 = (1 - iota((32, 128), 0) // 16) * HD
 
     sent(1, buf2.at[pl.ds(0, NKV - 1)])
+    for b in range(3):
+        d_v[b] = jnp.where(positions < lengths[b], d_v[b], MASKED)
     arrived(2, buf3.at[:, pl.ds(0, NTP - 1)])
     for b in range(3):
         qb = buf3[b].astype(BF16)
         s = dot(qb, k_v[b], NN) * (HD ** -0.5) + d_v[b]
-        live = positions < lengths[b]
-        s = jnp.where(live, s, MASKED)
-        top = jnp.max(s, axis=1, keepdims=True)
-        w = jnp.where(live, jnp.exp(s - top), 0.0)
+        top = jnp.maximum(jnp.max(s, axis=1, keepdims=True), 0.1 * MASKED)
+        w = jnp.exp(s - top)
         tot = jnp.sum(w, axis=1, keepdims=True)
         vs = dot(w.astype(BF16), v_v[b], NT)
         msg = jnp.where(ghalf32, vs, jnp.where(lane32 == mlane32, top, tot))
         stage4[b] = msg
+    send(3, "tp", (), lambda p: stage4.at[:, pl.ds(p, 1)], buf4.at[:, pl.ds(tp, 1)])
     buf4[:, pl.ds(tp, 1)] = stage4[:, pl.ds(tp, 1)]
-    send(3, "tp", (), lambda p: stage4.at[:, pl.ds(p, 1)], buf4.at[:, pl.ds(tp, 1)])
 
     def merge(y2):
         n = y2.shape[0]
@@ -304,12 +304,12 @@
     d_lo = (down - d_hi.astype(F32)).astype(BF16)
     parts = dot(fold, d_hi, NT) + dot(fold, d_lo, NT)
     parts = jnp.concatenate([parts, jnp.zeros((32, 64), F32)], axis=1)
-    stage8[...] = parts.reshape(32, 1, 128)
+    stage8[...] = parts
+    send(7, "tp", (), lambda p: stage8.at[pl.ds(p, 1)], buf8.at[pl.ds(tp, 1)])
     buf8[pl.ds(tp, 1)] = stage8[pl.ds(tp, 1)]
-    send(7, "tp", (), lambda p: stage8.at[p], buf8.at[tp])
     sent(6, buf7.at[pl.ds(0, NKV - 1)])
     arrived(7, buf8.at[pl.ds(0, NTP - 1)])
-    share = jnp.sum(buf8[...], axis=0)[:, :64] + res_mine
+    share = jnp.sum(buf8[...], axis=0, keepdims=True)[:, :64] + res_mine
     out[...] = jnp.concatenate([share[:, 0:8], share[:, 8:16], share[:, 16:24]], axis=0).astype(BF16)
     sent(7, buf8.at[pl.ds(0, NTP - 1)])
 
@@ -334,7 +334,7 @@
             v((NTP, 1, 128), F32), v((NKV, 8, 128), F32), v((3, NTP, 128), F32),
             v((3, NTP, 128), F32), v((3, NTP, 128), F32), v((3, NKV, 128), F32),
             v((NTP, 8, 128), BF16), v((NKV, 8, FF_PAD), BF16),
-            v((NTP, 1, 128), F32), v((NTP, 1, 128), F32),
+            v((NTP, 128), F32), v((NTP, 128), F32),
             pltpu.SemaphoreType.DMA((17,)),
             pltpu.SemaphoreType.DMA((8,)),
             pltpu.SemaphoreType.DMA((8,)),

time: 68.7 us -> 68.7 us (level)
  no operation moved by 1% of the time
where the time goes in v6:
time: 68.7 us; the launch traced here: 68.5 us
  Pallas kernels  68 us (99%)
    pallas_call x1, Pallas kernels, body(): pl.pallas_call(kernel, out_shape=pltpu.VMEM((3, 8), BF16), in_specs=[hbm]...  68 us

profile of v6, /device:TPU:1, one launch (start us, length us, event | category | flops | bytes accessed | tf_op | source)
XLA Modules:
  0.0 68.5 jit_solution(9284989776522196879)
XLA Ops:
  0.0 68.0 %shard_map.163 = bf16[3,8]{1,0:T(4,128)(2,1)S(1)} custom-call(s32[3]{0:T(128)} %lengths_h.1, bf16[3,8]{1,0:T(4,128)(2,1)} %tokens.1, f32[1,8]{1,0:T(1,128)} %bitcast.13, f32[1,8]{1,0:T(1,128)} %bitcast.14, f32[1,32]{1,0:T(1,128)} %bitcast.15, f32[16,128]{1,0:T(8,128)} %bitcast.12, bf16[64,256]{1,0:T(8,128)(2,1)} %bitcast.11, bf16[256,128]{1,0:T(8,128)(2,1)} %w_key.1, ...), custom_call_target="tpu_custom_call" | custom-call | tf_op jit(solution)/shard_map/pallas_call | solution.py:323
  68.0 0.6 copy.19
